TPU v7x, 32 devices: a whole 2x2x4 slice. The times are simulated.
32 devices in a mesh: ep: 32 (over z, y, x, core).
Axes of the slice: x: 2, y: 2, z: 4, core: 2. Of those that a mesh axis runs over, the one named last changes fastest.
Arguments:
- latest_embeddings: bfloat16 [512, 2048], P('ep'), may hold values from -6 to 6
- prior_memory_grids: float32 [512, 32, 4096], P('ep'), may hold values from -1.75 to 1.75
- earlier_rescale_gain: float32 [2048], replicated, may hold values from 0.1 to 1.9
- query_map: bfloat16 [2048, 2048], P(None, 'ep'), may hold values from -0.125 to 0.125
- lookup_map: bfloat16 [2048, 2048], P(None, 'ep'), may hold values from -0.125 to 0.125
- content_map: bfloat16 [2048, 2048], P(None, 'ep'), may hold values from -0.125 to 0.125
- forget_lower_map: bfloat16 [2048, 64], replicated, may hold values from -0.125 to 0.125
- forget_upper_map: bfloat16 [64, 2048], replicated, may hold values from -0.75 to 0.75
- forget_shift: float32 [2048], replicated, may hold values from -3 to 3
- adapt_lower_map: bfloat16 [2048, 64], replicated, may hold values from -0.125 to 0.125
- adapt_upper_map: bfloat16 [64, 2048], replicated, may hold values from -0.75 to 0.75
- adapt_shift: float32 [2048], replicated, may hold values from -2 to 2
- erase_lookup_gains: float32 [2048], replicated, may hold values from 0.1 to 1.9
- substitute_lookup_gains: float32 [2048], replicated, may hold values from 0.1 to 1.9
- present_extra_gains: float32 [2048], replicated, may hold values from -1.75 to 1.75
- attender_rescale_gain: float32 [2048], replicated, may hold values from 0.1 to 1.9
- result_map: bfloat16 [2048, 2048], P(None, 'ep'), may hold values from -0.125 to 0.125
- later_rescale_gain: float32 [2048], replicated, may hold values from 0.1 to 1.9
- specialist_switch_maps: bfloat16 [32, 2048, 512], P('ep'), may hold values from -0.125 to 0.125
- specialist_widen_maps: bfloat16 [32, 2048, 512], P('ep'), may hold values from -0.125 to 0.125
- specialist_shrink_maps: bfloat16 [32, 512, 2048], P('ep'), may hold values from -0.25 to 0.25
- picked_specialists: int32 [512, 6], P('ep'), may hold values from 0 to 31, as said below
- specialist_picked_shares: float32 [512, 6], P('ep'), may hold values from 0.02 to 0.5
Outputs:
- new_hidden: bfloat16 [512, 2048], P('ep')
- new_state: float32 [512, 32, 4096], P('ep')
Inputs may be any that keep to these rules, and one draw needn't show every extreme that they name: `picked_specialists`: each row names 6 different experts of one group; a group is a run of 8 consecutive expert numbers. The rows of one device use exactly two groups, one of them for half of the device's rows rounded up and the other for the rest. No expert is named by more than 6 rows of one device, and on every device some expert is named by exactly 6.
All inputs are finite; a program needn't handle non-finite values.
Results may differ from a plain program's by a relative error of at most 0.011.
Values may be sent and summed in bfloat16 or wider, within the bound.
A program may use at most 256 MiB of HBM per device.

v0:
```python
import math

import jax
import jax.numpy as jnp
from jax import lax
from jax.sharding import PartitionSpec as P

GROUPS = 4


norm_eps = 1e-06
group_eps = 0.00064
unit_eps = 1e-06


def rms_norm(rows_in, gain):
    values = rows_in.astype(jnp.float32)
    scale = lax.rsqrt(jnp.mean(values * values, axis=-1, keepdims=True) + norm_eps)
    return (values * scale * gain).astype(jnp.bfloat16)


def memory_readout(
    query_signal,
    substitute_lookup,
    content_signals,
    forget_multiplier,
    adapt_speed,
    erase_signal,
    memory_grid,
    attender_rescale_gain,
    present_extra_gains,
):
    highest = lax.Precision.HIGHEST
    removed = jnp.einsum("bhij,bhj->bhi", memory_grid, erase_signal, precision=highest)
    memory_grid = (
        memory_grid * forget_multiplier[:, :, None, :]
        - removed[..., None] * (erase_signal * adapt_speed)[:, :, None, :]
        + content_signals[..., None] * substitute_lookup[:, :, None, :]
    )
    readout = jnp.einsum("bhij,bhj->bhi", memory_grid, query_signal, precision=highest)
    centered = readout - jnp.mean(readout, axis=-1, keepdims=True)
    variance = jnp.mean(centered * centered, axis=-1, keepdims=True)
    rescaled_result = centered * lax.rsqrt(variance + group_eps) * attender_rescale_gain
    present_extra = (
        jnp.sum(query_signal * substitute_lookup * present_extra_gains, axis=-1, keepdims=True)
        * content_signals
    )
    return (rescaled_result + present_extra, memory_grid)


def local(
    latest_embeddings,
    prior_memory_grids,
    earlier_rescale_gain,
    query_map,
    lookup_map,
    content_map,
    forget_lower_map,
    forget_upper_map,
    forget_shift,
    adapt_lower_map,
    adapt_upper_map,
    adapt_shift,
    erase_lookup_gains,
    substitute_lookup_gains,
    present_extra_gains,
    attender_rescale_gain,
    result_map,
    later_rescale_gain,
    specialist_switch_maps,
    specialist_widen_maps,
    specialist_shrink_maps,
    picked_specialists,
    specialist_picked_shares,
):
    seq_count, model_width = latest_embeddings.shape
    attender_count = prior_memory_grids.shape[1]
    channel_span = model_width // attender_count
    devices = lax.axis_size("ep")
    columns = query_map.shape[1]
    normed = rms_norm(latest_embeddings, earlier_rescale_gain)
    stacked = jnp.concatenate([query_map, lookup_map, content_map], axis=1)
    projected = jnp.dot(
        lax.all_gather(normed, "ep", axis=0, tiled=True),
        stacked,
        preferred_element_type=jnp.float32,
    ).astype(jnp.bfloat16)
    query_signal, key_rows, content_signals = (
        lax.all_to_all(projected[:, :columns], "ep", split_axis=0, concat_axis=1, tiled=True),
        lax.all_to_all(
            projected[:, columns : 2 * columns], "ep", split_axis=0, concat_axis=1, tiled=True
        ),
        lax.all_to_all(projected[:, 2 * columns :], "ep", split_axis=0, concat_axis=1, tiled=True),
    )
    decay_low = jnp.tanh(
        jnp.dot(normed, forget_lower_map, preferred_element_type=jnp.float32)
    ).astype(jnp.bfloat16)
    forget_multiplier = jnp.exp(
        -math.exp(-0.5)
        * jax.nn.sigmoid(
            forget_shift + jnp.dot(decay_low, forget_upper_map, preferred_element_type=jnp.float32)
        )
    )
    rate_low = jnp.dot(normed, adapt_lower_map, preferred_element_type=jnp.float32).astype(
        jnp.bfloat16
    )
    adapt_speed = jax.nn.sigmoid(
        adapt_shift + jnp.dot(rate_low, adapt_upper_map, preferred_element_type=jnp.float32)
    )
    key_float = key_rows.astype(jnp.float32)
    erase_signal = (key_float * erase_lookup_gains).reshape(seq_count, attender_count, channel_span)
    erase_signal = erase_signal * lax.rsqrt(
        jnp.sum(erase_signal * erase_signal, axis=-1, keepdims=True) + unit_eps
    )
    substitute_lookup = key_float * (1.0 + (adapt_speed - 1.0) * substitute_lookup_gains)
    head_shape = (seq_count, attender_count, channel_span)
    mixed_heads, memory_grid = memory_readout(
        query_signal.astype(jnp.float32).reshape(head_shape),
        substitute_lookup.reshape(head_shape),
        content_signals.astype(jnp.float32).reshape(head_shape),
        forget_multiplier.reshape(head_shape),
        adapt_speed.reshape(head_shape),
        erase_signal,
        prior_memory_grids.reshape(seq_count, attender_count, channel_span, channel_span),
        attender_rescale_gain.reshape(attender_count, channel_span),
        present_extra_gains.reshape(attender_count, channel_span),
    )
    mixed = mixed_heads.reshape(seq_count, model_width).astype(jnp.bfloat16)
    new_state = memory_grid.reshape(seq_count, attender_count, channel_span * channel_span)
    partial_rows = jnp.dot(
        lax.all_gather(mixed, "ep", axis=0, tiled=True),
        result_map,
        preferred_element_type=jnp.float32,
    ).astype(jnp.bfloat16)
    mixer_out = lax.all_to_all(partial_rows, "ep", split_axis=0, concat_axis=1, tiled=True)
    residual = (latest_embeddings.astype(jnp.float32) + mixer_out.astype(jnp.float32)).astype(
        jnp.bfloat16
    )
    second = rms_norm(residual, later_rescale_gain)
    top_count = picked_specialists.shape[1]
    expert_count = specialist_switch_maps.shape[0] * devices
    group_size = expert_count // GROUPS
    capacity = ((seq_count + 1) // 2 * top_count + group_size - 1) // group_size
    flat_ids = picked_specialists.reshape(-1)
    matches = (flat_ids[:, None] == jnp.arange(expert_count, dtype=jnp.int32)[None, :]).astype(
        jnp.int32
    )
    slot_rank = jnp.sum((jnp.cumsum(matches, axis=0) - matches) * matches, axis=1)
    slot_ids = flat_ids * capacity + slot_rank
    picks = (
        slot_ids[:, None] == jnp.arange(expert_count * capacity, dtype=jnp.int32)[None, :]
    ).astype(jnp.bfloat16)
    repeated = jnp.repeat(second, top_count, axis=0)
    send_rows = jnp.einsum("sk,sd->kd", picks, repeated, preferred_element_type=jnp.float32).astype(
        jnp.bfloat16
    )
    send_rows = send_rows.reshape(devices, expert_count // devices * capacity, model_width)
    received = lax.all_to_all(send_rows, "ep", split_axis=0, concat_axis=0, tiled=True)
    rows_in = received.reshape(-1, model_width)
    gate_proj = jnp.dot(rows_in, specialist_switch_maps[0], preferred_element_type=jnp.float32)
    up_proj = jnp.dot(rows_in, specialist_widen_maps[0], preferred_element_type=jnp.float32)
    hidden_act = (jax.nn.silu(gate_proj) * up_proj).astype(jnp.bfloat16)
    results = jnp.dot(
        hidden_act, specialist_shrink_maps[0], preferred_element_type=jnp.float32
    ).astype(jnp.bfloat16)
    returned = lax.all_to_all(
        results.reshape(received.shape), "ep", split_axis=0, concat_axis=0, tiled=True
    )
    collected = jnp.dot(
        picks, returned.reshape(-1, model_width), preferred_element_type=jnp.float32
    )
    expert_sum = jnp.sum(
        collected.reshape(seq_count, top_count, model_width) * specialist_picked_shares[:, :, None],
        axis=1,
    )
    new_hidden = (residual.astype(jnp.float32) + expert_sum).astype(jnp.bfloat16)
    return (new_hidden, new_state)


def solution(mesh):
    return jax.shard_map(
        local,
        mesh=mesh,
        in_specs=(
            P("ep", None),
            P("ep", None, None),
            P(),
            P(None, "ep"),
            P(None, "ep"),
            P(None, "ep"),
            P(),
            P(),
            P(),
            P(),
            P(),
            P(),
            P(),
            P(),
            P(),
            P(),
            P(None, "ep"),
            P(),
            P("ep", None, None),
            P("ep", None, None),
            P("ep", None, None),
            P("ep", None),
            P("ep", None),
        ),
        out_specs=(P("ep", None), P("ep", None, None)),
        check_vma=False,
    )
```

profile of v0, /device:TPU:15, one launch (start us, length us, event | category | flops | bytes accessed | tf_op | source)
XLA Modules:
  0.0 338.2 jit_solution(15131973935184943869)
XLA Ops:
  8.3 1.6 fusion.59
  12.2 55.2 %all-gather.3.cloned.1.call-done = bf16[512,2048]{1,0:T(8,128)(2,1)} async-done(((bf16[16,2048]{1,0:T(8,128)(2,1)}), bf16[512,2048]{1,0:T(8,128)(2,1)}) %all-gather.3.cloned.1.call-update) | async-done | bytes 2097168 | tf_op jit(solution)/shard_map/all_gather | solution.py:84
  67.4 2.6 convolution_convert_fusion.2
  71.0 5.3 %all-to-all-start = ((bf16[32,2,512]{2,1,0:T(2,128)(2,1)}), bf16[32,2,512]{2,1,0:T(2,128)(2,1)S(1)}, u32[]{:S(2)}, u32[]{:S(2)}) async-start(bf16[32,2,512]{2,1,0:T(2,128)(2,1)} %reshape.162), calls=%async_computation | async-start | bytes 131072 | tf_op jit(solution)/shard_map/all_to_all | solution.py:90
  76.3 1.5 fusion.15
  77.9 14.2 %reshape.147 = f32[16,32,64,64]{3,2,1,0:T(8,128)} reshape(f32[16,32,4096]{2,1,0:T(8,128)} %param.24) | data formatting | bytes 16777216 | tf_op jit(solution)/shard_map/reshape | solution.py:124
  93.9 5.8 %all-to-all-start.1 = ((bf16[32,2,512]{2,1,0:T(2,128)(2,1)}), bf16[32,2,512]{2,1,0:T(2,128)(2,1)S(1)}, u32[]{:S(2)}, u32[]{:S(2)}) async-start(bf16[32,2,512]{2,1,0:T(2,128)(2,1)} %reshape.164), calls=%async_computation.1 | async-start | bytes 131072 | tf_op jit(solution)/shard_map/all_to_all | solution.py:93
  100.3 1.4 add_multiply_fusion
  102.7 28.7 %fusion.51 = f32[16,32,1,64]{3,2,1,0:T(1,128)S(1)} fusion(f32[16,32,64,64]{3,2,1,0:T(8,128)} %reshape.147, f32[16,32,64,1]{2,0,1,3:T(8,128)S(1)} %get-tuple-element.7), kind=kOutput, calls=%fused_computation.61 | convolution fusion | flops 25165824 | bytes 8650752 | tf_op jit(solution)/shard_map/bhij,bhj->bhi/dot_general | solution.py:34
  132.6 5.8 %all-to-all-start.2 = ((bf16[32,2,512]{2,1,0:T(2,128)(2,1)}), bf16[32,2,512]{2,1,0:T(2,128)(2,1)S(1)}, u32[]{:S(2)}, u32[]{:S(2)}) async-start(bf16[32,2,512]{2,1,0:T(2,128)(2,1)} %reshape.166), calls=%async_computation.2 | async-start | bytes 131072 | tf_op jit(solution)/shard_map/all_to_all | solution.py:89
  139.6 3.3 all-to-all-done.2
  143.1 20.5 %fusion.1 = f32[16,32,1,64]{3,2,1,0:T(1,128)S(1)} fusion(f32[16,32,64,64]{3,2,1,0:T(8,128)} %reshape.147, f32[16,32,64]{2,1,0:T(8,128)S(1)} %mul.216, f32[16,32,64]{2,1,0:T(8,128)S(1)} %copy.61, f32[16,32,64]{2,1,0:T(8,128)S(1)} %bitcast.81, f32[16,32,64]{2,1,0:T(8,128)S(1)} %mul.234, f32[16,32,64]{2,1,0:T(8,128)} %copy.63, ...), kind=kOutput, calls=%fused_computation.1 | convolution fusion | flops 35651584 | bytes 9240576 | tf_op jit(solution)/shard_map/bhij,bhj->bhi/dot_general | solution.py:40
  166.8 6.8 %mul.217 = f32[16,32,64,64]{3,2,1,0:T(8,128)} broadcast(f32[16,32,64]{2,1,0:T(8,128)S(1)} %mul.216), dimensions={0,1,3} | broadcast | bytes 8519680 | tf_op jit(solution)/shard_map/mul | solution.py:36
  173.6 14.8 %mul.263 = f32[16,32,4096]{2,1,0:T(8,128)} reshape(f32[16,32,64,64]{3,2,1,0:T(8,128)} %mul.217) | data formatting | bytes 16777216 | tf_op jit(solution)/shard_map/mul | solution.py:36
  188.5 31.7 %all-gather.5.cloned.1.call-done = bf16[512,2048]{1,0:T(8,128)(2,1)} async-done(((bf16[16,2048]{1,0:T(8,128)(2,1)}), bf16[512,2048]{1,0:T(8,128)(2,1)}) %all-gather.5.cloned.1.call-update) | async-done | bytes 2097168 | tf_op jit(solution)/shard_map/all_gather | solution.py:131
  220.2 2.3 convolution_convert_fusion.3
  223.4 5.3 %all-to-all-start.3 = ((bf16[32,2,512]{2,1,0:T(2,128)(2,1)}), bf16[32,2,512]{2,1,0:T(2,128)(2,1)S(1)}, u32[]{:S(2)}, u32[]{:S(2)}) async-start(bf16[32,2,512]{2,1,0:T(2,128)(2,1)} %reshape.168), calls=%async_computation.3 | async-start | bytes 131072 | tf_op jit(solution)/shard_map/all_to_all | solution.py:135
  228.7 4.5 %all-to-all-done.3 = bf16[32,2,512]{2,1,0:T(2,128)(2,1)S(1)} async-done(((bf16[32,2,512]{2,1,0:T(2,128)(2,1)}), bf16[32,2,512]{2,1,0:T(2,128)(2,1)S(1)}, u32[]{:S(2)}, u32[]{:S(2)}) %all-to-all-start.3) | async-done | bytes 65568 | tf_op jit(solution)/shard_map/all_to_all | solution.py:135
  234.8 1.5 convolution_convert_fusion.1
  236.3 1.2 reshape.150
  237.5 5.5 %all-to-all-start.4 = ((bf16[32,6,2048]{2,1,0:T(8,128)(2,1)}), bf16[32,6,2048]{2,1,0:T(8,128)(2,1)S(1)}, u32[]{:S(2)}, u32[]{:S(2)}) async-start(bf16[32,6,2048]{2,1,0:T(8,128)(2,1)} %reshape.150), calls=%async_computation.4 | async-start | bytes 2097152 | tf_op jit(solution)/shard_map/all_to_all | solution.py:158
  243.1 9.3 %broadcast_multiply_fusion = f32[16,32,64,64]{3,2,1,0:T(8,128)} fusion(f32[16,32,64]{2,1,0:T(8,128)S(1)} %mul.234, f32[16,32,64]{2,1,0:T(8,128)} %copy.63), kind=kLoop, calls=%fused_computation.6 | loop fusion | flops 2097152 | bytes 8650752 | tf_op jit(solution)/shard_map/mul | solution.py:38
  252.4 14.8 %mul.266 = f32[16,32,4096]{2,1,0:T(8,128)} reshape(f32[16,32,64,64]{3,2,1,0:T(8,128)} %broadcast_multiply_fusion) | data formatting | bytes 16777216 | tf_op jit(solution)/shard_map/mul | solution.py:38
  267.2 9.3 %broadcast_multiply_fusion.1 = f32[16,32,64,64]{3,2,1,0:T(8,128)} fusion(f32[16,32,64]{2,1,0:T(8,128)} %copy-done.3, f32[16,32,64]{2,1,0:T(8,128)S(1)} %bitcast.82), kind=kLoop, calls=%fused_computation.7 | loop fusion | flops 2097152 | bytes 8650752 | tf_op jit(solution)/shard_map/mul | solution.py:37
  276.5 14.7 %mul.265 = f32[16,32,4096]{2,1,0:T(8,128)} reshape(f32[16,32,64,64]{3,2,1,0:T(8,128)} %broadcast_multiply_fusion.1) | data formatting | bytes 16777216 | tf_op jit(solution)/shard_map/mul | solution.py:37
  292.4 2.4 fusion.19
  294.8 3.0 convolution_convert_fusion
  297.8 1.2 reshape.152
  299.0 5.9 %all-to-all-start.5 = ((bf16[32,6,2048]{2,1,0:T(8,128)(2,1)}), bf16[32,6,2048]{2,1,0:T(8,128)(2,1)S(1)}, u32[]{:S(2)}, u32[]{:S(2)}) async-start(bf16[32,6,2048]{2,1,0:T(8,128)(2,1)} %reshape.152), calls=%async_computation.5 | async-start | bytes 2097152 | tf_op jit(solution)/shard_map/all_to_all | solution.py:166
  304.9 16.1 %subtract_add_fusion = f32[16,32,4096]{2,1,0:T(8,128)} fusion(f32[16,32,4096]{2,1,0:T(8,128)} %mul.266, f32[16,32,4096]{2,1,0:T(8,128)} %mul.265, f32[16,32,4096]{2,1,0:T(8,128)} %param.24, f32[16,32,4096]{2,1,0:T(8,128)} %mul.263), kind=kLoop, calls=%fused_computation.5 | loop fusion | flops 6291456 | bytes 41943040 | tf_op jit(solution)/shard_map/add | solution.py:36
  321.0 7.1 %all-to-all-done.5 = bf16[32,6,2048]{2,1,0:T(8,128)(2,1)S(1)} async-done(((bf16[32,6,2048]{2,1,0:T(8,128)(2,1)}), bf16[32,6,2048]{2,1,0:T(8,128)(2,1)S(1)}, u32[]{:S(2)}, u32[]{:S(2)}) %all-to-all-start.5) | async-done | bytes 786464 | tf_op jit(solution)/shard_map/all_to_all | solution.py:166
  329.2 1.5 fusion.21
  (90 shorter events, 18.8 us)
Async XLA Ops:
  7.2 287.7 %copy-start = (bf16[1,512,2048]{2,1,0:T(8,128)(2,1)S(1)}, bf16[1,512,2048]{2,1,0:T(8,128)(2,1)}, u32[]{:S(2)}) copy-start(bf16[1,512,2048]{2,1,0:T(8,128)(2,1)} %param.43) | copy-start | bytes 6291460
  7.2 60.3 %all-gather.3.cloned.1.call-start = ((), (), s32[]{:S(2)}) async-start(), calls=%async_computation.6 | async-start | bytes 2162688 | tf_op jit(solution)/shard_map/all_gather | solution.py:84
  71.0 23.0 %all-to-all-start = ((bf16[32,2,512]{2,1,0:T(2,128)(2,1)}), bf16[32,2,512]{2,1,0:T(2,128)(2,1)S(1)}, u32[]{:S(2)}, u32[]{:S(2)}) async-start(bf16[32,2,512]{2,1,0:T(2,128)(2,1)} %reshape.162), calls=%async_computation | async-start | bytes 131072 | tf_op jit(solution)/shard_map/all_to_all | solution.py:90
  77.9 22.4 %copy-start.6 = (bf16[16,2048]{1,0:T(8,128)(2,1)S(1)}, bf16[16,2048]{1,0:T(8,128)(2,1)}, u32[]{:S(2)}) copy-start(bf16[16,2048]{1,0:T(8,128)(2,1)} %fusion.59) | copy-start | bytes 196612
  77.9 22.4 %copy-start.9 = (bf16[64,2048]{1,0:T(8,128)(2,1)S(1)}, bf16[64,2048]{1,0:T(8,128)(2,1)}, u32[]{:S(2)}) copy-start(bf16[64,2048]{1,0:T(8,128)(2,1)} %param.33) | copy-start | bytes 786436
  77.9 22.4 %copy-start.10 = (f32[2048]{0:T(1024)S(1)}, f32[2048]{0:T(1024)}, u32[]{:S(2)}) copy-start(f32[2048]{0:T(1024)} %param.36) | copy-start | bytes 24580
  77.9 22.4 %copy-start.11 = (f32[2048]{0:T(1024)S(1)}, f32[2048]{0:T(1024)}, u32[]{:S(2)}) copy-start(f32[2048]{0:T(1024)} %param.34) | copy-start | bytes 24580
  93.9 38.6 %all-to-all-start.1 = ((bf16[32,2,512]{2,1,0:T(2,128)(2,1)}), bf16[32,2,512]{2,1,0:T(2,128)(2,1)S(1)}, u32[]{:S(2)}, u32[]{:S(2)}) async-start(bf16[32,2,512]{2,1,0:T(2,128)(2,1)} %reshape.164), calls=%async_computation.1 | async-start | bytes 131072 | tf_op jit(solution)/shard_map/all_to_all | solution.py:93
  131.4 32.2 %copy-start.1 = (f32[16,32,1,64]{3,2,1,0:T(1,128)}, f32[16,32,1,64]{3,2,1,0:T(1,128)S(1)}, u32[]{:S(2)}) copy-start(f32[16,32,1,64]{3,2,1,0:T(1,128)S(1)} %fusion.51) | copy-start | bytes 393220
  132.5 31.0 %copy-start.3 = (f32[16,32,64]{2,1,0:T(8,128)}, f32[16,32,64]{2,1,0:T(8,128)S(1)}, u32[]{:S(2)}) copy-start(f32[16,32,64]{2,1,0:T(8,128)S(1)} %copy.61) | copy-start | bytes 393220
  132.6 10.3 %all-to-all-start.2 = ((bf16[32,2,512]{2,1,0:T(2,128)(2,1)}), bf16[32,2,512]{2,1,0:T(2,128)(2,1)S(1)}, u32[]{:S(2)}, u32[]{:S(2)}) async-start(bf16[32,2,512]{2,1,0:T(2,128)(2,1)} %reshape.166), calls=%async_computation.2 | async-start | bytes 131072 | tf_op jit(solution)/shard_map/all_to_all | solution.py:89
  138.4 81.8 %all-gather.5.cloned.1.call-start = ((), (), s32[]{:S(2)}) async-start(), calls=%async_computation.7 | async-start | bytes 2162688 | tf_op jit(solution)/shard_map/all_gather | solution.py:131
  143.0 23.0 %copy-start.7 = (s32[16,6]{0,1:T(8,128)S(1)}, s32[16,6]{0,1:T(8,128)}, u32[]{:S(2)}) copy-start(s32[16,6]{0,1:T(8,128)} %param.44) | copy-start | bytes 1156
  173.6 46.6 %copy-start.5 = (bf16[2048,64]{0,1:T(8,128)(2,1)S(1)}, bf16[2048,64]{0,1:T(8,128)(2,1)}, u32[]{:S(2)}) copy-start(bf16[2048,64]{0,1:T(8,128)(2,1)} %param.39) | copy-start | bytes 786436
  173.6 60.0 %copy-start.4 = (bf16[16,2048]{1,0:T(8,128)(2,1)S(1)}, bf16[16,2048]{1,0:T(8,128)(2,1)}, u32[]{:S(2)}) copy-start(bf16[16,2048]{1,0:T(8,128)(2,1)} %param.23) | copy-start | bytes 196612
  173.6 60.2 %copy-start.8 = (f32[2048]{0:T(1024)S(1)}, f32[2048]{0:T(1024)}, u32[]{:S(2)}) copy-start(f32[2048]{0:T(1024)} %param.40) | copy-start | bytes 24580
  223.4 9.8 %all-to-all-start.3 = ((bf16[32,2,512]{2,1,0:T(2,128)(2,1)}), bf16[32,2,512]{2,1,0:T(2,128)(2,1)S(1)}, u32[]{:S(2)}, u32[]{:S(2)}) async-start(bf16[32,2,512]{2,1,0:T(2,128)(2,1)} %reshape.168), calls=%async_computation.3 | async-start | bytes 131072 | tf_op jit(solution)/shard_map/all_to_all | solution.py:135
  237.5 53.7 %all-to-all-start.4 = ((bf16[32,6,2048]{2,1,0:T(8,128)(2,1)}), bf16[32,6,2048]{2,1,0:T(8,128)(2,1)S(1)}, u32[]{:S(2)}, u32[]{:S(2)}) async-start(bf16[32,6,2048]{2,1,0:T(8,128)(2,1)} %reshape.150), calls=%async_computation.4 | async-start | bytes 2097152 | tf_op jit(solution)/shard_map/all_to_all | solution.py:158
  252.4 14.8 %copy-start.2 = (f32[16,32,1,64]{3,2,1,0:T(1,128)S(1)}, f32[16,32,1,64]{3,2,1,0:T(1,128)}, u32[]{:S(2)}) copy-start(f32[16,32,1,64]{3,2,1,0:T(1,128)} %copy-done.1) | copy-start | bytes 393220
  299.0 29.0 %all-to-all-start.5 = ((bf16[32,6,2048]{2,1,0:T(8,128)(2,1)}), bf16[32,6,2048]{2,1,0:T(8,128)(2,1)S(1)}, u32[]{:S(2)}, u32[]{:S(2)}) async-start(bf16[32,6,2048]{2,1,0:T(8,128)(2,1)} %reshape.152), calls=%async_computation.5 | async-start | bytes 2097152 | tf_op jit(solution)/shard_map/all_to_all | solution.py:166
  304.9 24.3 %copy-start.12 = (f32[16,6]{0,1:T(8,128)S(1)}, f32[16,6]{0,1:T(8,128)}, u32[]{:S(2)}) copy-start(f32[16,6]{0,1:T(8,128)} %param.45) | copy-start | bytes 1156
Sparse Core Ops, SparseCore 0:
  11.4 55.9 all-gather.2
  166.1 54.0 all-gather.4
where the time goes:
time: 345 us; the launch traced here: 338 us
  waiting for transfers between devices  102 us (30%)
  local copies, waits for them, and re-layouts  81.3 us (24%)
  matrix products  65.2 us (19%)
  other arithmetic  41.3 us (12%)
  starting transfers between devices  33.9 us (10%)
  between operations  14.5 us (4%)
    all_gather x1, waiting for transfers between devices, local(): lax.all_gather(normed, 'ep', axis=0, tiled=True)  55.2 us
    all_gather x1, waiting for transfers between devices, local(): lax.all_gather(mixed, 'ep', axis=0, tiled=True)  31.7 us
    dot_general x1, matrix products, memory_readout(): jnp.einsum('bhij,bhj->bhi', memory_grid, erase_signal, precision=highest)  28.7 us
    mul x3, local copies, waits for them, and re-layouts, memory_readout(): memory_grid * forget_multiplier[:, :, None, :]  21.8 us
    dot_general x1, matrix products, memory_readout(): jnp.einsum('bhij,bhj->bhi', memory_grid, query_signal, precision=highest)  20.5 us
    add x1, other arithmetic, memory_readout(): memory_grid * forget_multiplier[:, :, None, :]  16.1 us
    mul x2, local copies, waits for them, and re-layouts, memory_readout(): content_signals[..., None] * substitute_lookup[:, :, None, :]  14.9 us
    mul x1, local copies, waits for them, and re-layouts, memory_readout(): removed[..., None] * (erase_signal * adapt_speed)[:, :, None, :]  14.7 us
  transfers between devices with their start and end apart: 8, of which 5 were waited for; matrix products, arithmetic and copies ran while one was open for 41% of the time, Pallas kernels for 0%

commit v1 on v0

v1 whole, which is shorter than its diff:
```python
import functools
import math

import jax
import jax.numpy as jnp
from jax import lax
from jax.experimental import pallas as pl
from jax.experimental.pallas import tpu as pltpu
from jax.sharding import PartitionSpec as P

GROUPS = 4
MESH = pl.DeviceIdType.MESH

norm_eps = 1e-06
group_eps = 0.00064
unit_eps = 1e-06


def rms_norm(rows_in, gain):
    values = rows_in.astype(jnp.float32)
    scale = lax.rsqrt(jnp.mean(values * values, axis=-1, keepdims=True) + norm_eps)
    return (values * scale * gain).astype(jnp.bfloat16)


def state_kernel(
    q_ref, k_ref, v_ref, dl_ref, al_ref, eg_ref, sg_ref, xg_ref, ag_ref, m_ref,
    mixed_ref, out_ref, sum_ref, spread_ref,
):
    rows, span = q_ref.shape
    repeat = rows // eg_ref.shape[0]
    width = 4 * span
    chunks = m_ref.shape[1] // width
    f32, bf16 = jnp.float32, jnp.bfloat16

    @pl.when(pl.program_id(0) == 0)
    def _():
        shape = sum_ref.shape
        sum_ref[...] = jnp.where(
            lax.broadcasted_iota(jnp.int32, shape, 0) // span
            == lax.broadcasted_iota(jnp.int32, shape, 1),
            1.0, 0.0,
        ).astype(bf16)
        shape = spread_ref.shape
        spread_ref[...] = jnp.where(
            lax.broadcasted_iota(jnp.int32, shape, 1) // span
            == lax.broadcasted_iota(jnp.int32, shape, 0) % span,
            1.0, 0.0,
        ).astype(bf16)

    def gains(ref):
        return jnp.concatenate([ref[...]] * repeat, axis=0)

    def wide(x):
        return jnp.concatenate([x] * 4, axis=1)

    def head_sum(x):
        return jnp.sum(x, axis=-1, keepdims=True)

    q = q_ref[...].astype(f32)
    k = k_ref[...].astype(f32)
    v16 = v_ref[...]
    v = v16.astype(f32)
    decay = jnp.exp(-math.exp(-0.5) * jax.nn.sigmoid(dl_ref[...]))
    rate = jax.nn.sigmoid(al_ref[...])
    erase = k * gains(eg_ref)
    erase = erase * lax.rsqrt(head_sum(erase * erase) + unit_eps)
    repl = k * (1.0 + (rate - 1.0) * gains(sg_ref))
    erase_rate = erase * rate
    erase_w, decay_w, query_w = wide(erase), wide(decay), wide(decay * q)
    removed = jnp.zeros((rows, span), f32)
    kept = jnp.zeros((rows, span), f32)
    for c in range(chunks):
        part = pl.ds(c * width, width)
        m = m_ref[:, part]
        picker = sum_ref[part, :]
        removed += jnp.dot((m * erase_w).astype(bf16), picker, preferred_element_type=f32)
        kept += jnp.dot((m * query_w).astype(bf16), picker, preferred_element_type=f32)
    readout = kept - removed * head_sum(erase_rate * q) + v * head_sum(repl * q)
    centered = readout - jnp.mean(readout, axis=-1, keepdims=True)
    variance = jnp.mean(centered * centered, axis=-1, keepdims=True)
    mixed = centered * lax.rsqrt(variance + group_eps) * gains(ag_ref)
    mixed_ref[...] = (mixed + head_sum(q * repl * gains(xg_ref)) * v).astype(bf16)
    high = removed.astype(bf16)
    low = (removed - high.astype(f32)).astype(bf16)
    both = jnp.concatenate([high, low], axis=1)
    rate_w, repl_w = wide(erase_rate), wide(repl)
    for c in range(chunks):
        part = pl.ds(c * width, width)
        gone = jnp.dot(both, spread_ref[:, part], preferred_element_type=f32)
        added = jnp.dot(v16, spread_ref[:span, part], preferred_element_type=f32)
        out_ref[:, part] = m_ref[:, part] * decay_w - gone * rate_w + added * repl_w


def update_state(q, k, v, decay_logit, rate_logit, gains, state):
    seqs, heads, cells = state.shape
    span = q.shape[1]
    block = 2 * heads
    row = pl.BlockSpec((block, span), lambda i: (i, 0))
    gain = pl.BlockSpec((heads, span), lambda i: (0, 0))
    big = pl.BlockSpec((block, cells), lambda i: (i, 0))
    mixed, new = pl.pallas_call(
        state_kernel,
        grid=(seqs * heads // block,),
        in_specs=[row] * 5 + [gain] * 4 + [big],
        out_specs=[row, big],
        out_shape=[
            jax.ShapeDtypeStruct((seqs * heads, span), jnp.bfloat16),
            jax.ShapeDtypeStruct((seqs * heads, cells), jnp.float32),
        ],
        scratch_shapes=[
            pltpu.VMEM((cells, span), jnp.bfloat16),
            pltpu.VMEM((2 * span, cells), jnp.bfloat16),
        ],
        compiler_params=pltpu.CompilerParams(vmem_limit_bytes=40 * 2**20),
        name="state",
    )(q, k, v, decay_logit, rate_logit, *gains, state.reshape(seqs * heads, cells))
    return mixed, new.reshape(state.shape)


def project_kernel(
    devices, x_ref, w_ref, out_ref, gathered, other, result, landed,
    x_send, x_recv, r_send, r_recv, w_send, w_recv, local_sem,
):
    me = lax.axis_index("ep")
    core, chip = me % 2, me // 2
    partner = me + 1 - 2 * core
    chips = devices // 2
    rows = x_ref.shape[0]
    barrier = pltpu.get_barrier_semaphore()
    pl.semaphore_signal(barrier, inc=1, device_id=(partner,), device_id_type=MESH)

    def greet(k, carry):
        pl.semaphore_signal(
            barrier, inc=1, device_id=((me + 2 * k) % devices,), device_id_type=MESH
        )
        return carry

    lax.fori_loop(1, chips, greet, 0)
    pl.semaphore_wait(barrier, chips)

    def token_copy(k):
        return pltpu.make_async_remote_copy(
            src_ref=x_ref,
            dst_ref=gathered.at[chip],
            send_sem=x_send.at[k],
            recv_sem=x_recv.at[k],
            device_id=((me + 2 * k) % devices,),
            device_id_type=MESH,
        )

    def result_copy(k):
        peer = (me + 2 * k) % devices
        return pltpu.make_async_remote_copy(
            src_ref=result.at[peer // 2],
            dst_ref=landed.at[chip],
            send_sem=r_send.at[k],
            recv_sem=r_recv.at[k],
            device_id=(peer,),
            device_id_type=MESH,
        )

    def start(make):
        def step(k, carry):
            make(k).start()
            return carry
        lax.fori_loop(1, chips, step, 0)

    def finish(make):
        def step(k, carry):
            make(k).wait()
            return carry
        lax.fori_loop(1, chips, step, 0)

    weights = pltpu.make_async_remote_copy(
        src_ref=w_ref,
        dst_ref=other,
        send_sem=w_send,
        recv_sem=w_recv,
        device_id=(partner,),
        device_id_type=MESH,
    )
    start(token_copy)
    weights.start()
    mine = pltpu.make_async_copy(x_ref, gathered.at[chip], local_sem)
    mine.start()
    mine.wait()
    weights.wait()
    finish(token_copy)
    tokens = gathered[...].reshape(chips * rows, x_ref.shape[1])
    for ref, at in ((w_ref, core), (other, 1 - core)):
        product = jnp.dot(tokens, ref[...], preferred_element_type=jnp.float32)
        product = product.astype(jnp.bfloat16)
        for c in range(chips):
            result[c, at] = product[c * rows : (c + 1) * rows]
    start(result_copy)
    mine = pltpu.make_async_copy(result.at[chip], landed.at[chip], local_sem)
    mine.start()
    mine.wait()
    finish(result_copy)
    out_ref[...] = landed[...]


def project(x, w, ident):
    devices = lax.axis_size("ep")
    chips = devices // 2
    rows, depth = x.shape
    columns = w.shape[1]
    shape = (chips, 2, rows, columns)
    out = pl.pallas_call(
        functools.partial(project_kernel, devices),
        out_shape=jax.ShapeDtypeStruct(shape, jnp.bfloat16),
        in_specs=[pl.BlockSpec(memory_space=pltpu.VMEM)] * 2,
        out_specs=pl.BlockSpec(memory_space=pltpu.VMEM),
        scratch_shapes=[
            pltpu.VMEM((chips, rows, depth), jnp.bfloat16),
            pltpu.VMEM(w.shape, jnp.bfloat16),
            pltpu.VMEM(shape, jnp.bfloat16),
            pltpu.VMEM(shape, jnp.bfloat16),
            pltpu.SemaphoreType.DMA((chips,)),
            pltpu.SemaphoreType.DMA((chips,)),
            pltpu.SemaphoreType.DMA((chips,)),
            pltpu.SemaphoreType.DMA((chips,)),
            pltpu.SemaphoreType.DMA,
            pltpu.SemaphoreType.DMA,
            pltpu.SemaphoreType.DMA,
        ],
        compiler_params=pltpu.CompilerParams(
            collective_id=ident, has_side_effects=True, vmem_limit_bytes=50 * 2**20
        ),
        name=f"project{ident}",
    )(x, w)
    return out.reshape(devices, rows, columns)


def exchange_kernel(devices, x_ref, out_ref, landed, send_sem, recv_sem, local_sem):
    me = lax.axis_index("ep")
    barrier = pltpu.get_barrier_semaphore()

    def greet(k, carry):
        pl.semaphore_signal(
            barrier, inc=1, device_id=((me + k) % devices,), device_id_type=MESH
        )
        return carry

    lax.fori_loop(1, devices, greet, 0)
    pl.semaphore_wait(barrier, devices - 1)

    def copy(k):
        peer = (me + k) % devices
        return pltpu.make_async_remote_copy(
            src_ref=x_ref.at[peer],
            dst_ref=landed.at[me],
            send_sem=send_sem.at[k],
            recv_sem=recv_sem.at[k],
            device_id=(peer,),
            device_id_type=MESH,
        )

    def start(k, carry):
        copy(k).start()
        return carry

    def finish(k, carry):
        copy(k).wait()
        return carry

    lax.fori_loop(1, devices, start, 0)
    mine = pltpu.make_async_copy(x_ref.at[me], landed.at[me], local_sem)
    mine.start()
    mine.wait()
    lax.fori_loop(1, devices, finish, 0)
    out_ref[...] = landed[...]


def exchange(x, ident):
    devices = lax.axis_size("ep")
    blocks = x.reshape(devices, -1, 128)
    out = pl.pallas_call(
        functools.partial(exchange_kernel, devices),
        out_shape=jax.ShapeDtypeStruct(blocks.shape, x.dtype),
        in_specs=[pl.BlockSpec(memory_space=pltpu.VMEM)],
        out_specs=pl.BlockSpec(memory_space=pltpu.VMEM),
        scratch_shapes=[
            pltpu.VMEM(blocks.shape, x.dtype),
            pltpu.SemaphoreType.DMA((devices,)),
            pltpu.SemaphoreType.DMA((devices,)),
            pltpu.SemaphoreType.DMA,
        ],
        compiler_params=pltpu.CompilerParams(collective_id=ident, has_side_effects=True),
        name=f"exchange{ident}",
    )(blocks)
    return out.reshape(x.shape)


def local(
    latest_embeddings,
    prior_memory_grids,
    earlier_rescale_gain,
    query_map,
    lookup_map,
    content_map,
    forget_lower_map,
    forget_upper_map,
    forget_shift,
    adapt_lower_map,
    adapt_upper_map,
    adapt_shift,
    erase_lookup_gains,
    substitute_lookup_gains,
    present_extra_gains,
    attender_rescale_gain,
    result_map,
    later_rescale_gain,
    specialist_switch_maps,
    specialist_widen_maps,
    specialist_shrink_maps,
    picked_specialists,
    specialist_picked_shares,
):
    seq_count, model_width = latest_embeddings.shape
    attender_count = prior_memory_grids.shape[1]
    channel_span = model_width // attender_count
    devices = lax.axis_size("ep")
    columns = query_map.shape[1]
    normed = rms_norm(latest_embeddings, earlier_rescale_gain)
    stacked = jnp.concatenate([query_map, lookup_map, content_map], axis=1)
    projected = project(normed, stacked, 0).reshape(devices, seq_count, 3, columns)
    projected = projected.transpose(2, 1, 0, 3).reshape(
        3, seq_count * attender_count, channel_span
    )
    decay_low = jnp.tanh(
        jnp.dot(normed, forget_lower_map, preferred_element_type=jnp.float32)
    ).astype(jnp.bfloat16)
    decay_logit = forget_shift + jnp.dot(
        decay_low, forget_upper_map, preferred_element_type=jnp.float32
    )
    rate_low = jnp.dot(normed, adapt_lower_map, preferred_element_type=jnp.float32).astype(
        jnp.bfloat16
    )
    rate_logit = adapt_shift + jnp.dot(
        rate_low, adapt_upper_map, preferred_element_type=jnp.float32
    )
    mixed, new_state = update_state(
        projected[0],
        projected[1],
        projected[2],
        decay_logit.reshape(-1, channel_span),
        rate_logit.reshape(-1, channel_span),
        [
            gain.reshape(attender_count, channel_span)
            for gain in (
                erase_lookup_gains,
                substitute_lookup_gains,
                present_extra_gains,
                attender_rescale_gain,
            )
        ],
        prior_memory_grids,
    )
    mixer_out = project(mixed.reshape(seq_count, model_width), result_map, 1)
    mixer_out = mixer_out.transpose(1, 0, 2).reshape(seq_count, model_width)
    residual = (latest_embeddings.astype(jnp.float32) + mixer_out.astype(jnp.float32)).astype(
        jnp.bfloat16
    )
    second = rms_norm(residual, later_rescale_gain)
    top_count = picked_specialists.shape[1]
    expert_count = specialist_switch_maps.shape[0] * devices
    group_size = expert_count // GROUPS
    capacity = ((seq_count + 1) // 2 * top_count + group_size - 1) // group_size
    flat_ids = picked_specialists.reshape(-1)
    matches = (flat_ids[:, None] == jnp.arange(expert_count, dtype=jnp.int32)[None, :]).astype(
        jnp.int32
    )
    slot_rank = jnp.sum((jnp.cumsum(matches, axis=0) - matches) * matches, axis=1)
    slot_ids = flat_ids * capacity + slot_rank
    picks = (
        slot_ids[:, None] == jnp.arange(expert_count * capacity, dtype=jnp.int32)[None, :]
    ).astype(jnp.bfloat16)
    repeated = jnp.repeat(second, top_count, axis=0)
    send_rows = jnp.einsum("sk,sd->kd", picks, repeated, preferred_element_type=jnp.float32).astype(
        jnp.bfloat16
    )
    send_rows = send_rows.reshape(devices, expert_count // devices * capacity, model_width)
    received = exchange(send_rows, 2)
    rows_in = received.reshape(-1, model_width)
    gate_proj = jnp.dot(rows_in, specialist_switch_maps[0], preferred_element_type=jnp.float32)
    up_proj = jnp.dot(rows_in, specialist_widen_maps[0], preferred_element_type=jnp.float32)
    hidden_act = (jax.nn.silu(gate_proj) * up_proj).astype(jnp.bfloat16)
    results = jnp.dot(
        hidden_act, specialist_shrink_maps[0], preferred_element_type=jnp.float32
    ).astype(jnp.bfloat16)
    returned = exchange(results.reshape(received.shape), 3)
    collected = jnp.dot(
        picks, returned.reshape(-1, model_width), preferred_element_type=jnp.float32
    )
    expert_sum = jnp.sum(
        collected.reshape(seq_count, top_count, model_width) * specialist_picked_shares[:, :, None],
        axis=1,
    )
    new_hidden = (residual.astype(jnp.float32) + expert_sum).astype(jnp.bfloat16)
    return (new_hidden, new_state)


def solution(mesh):
    return jax.shard_map(
        local,
        mesh=mesh,
        in_specs=(
            P("ep", None),
            P("ep", None, None),
            P(),
            P(None, "ep"),
            P(None, "ep"),
            P(None, "ep"),
            P(),
            P(),
            P(),
            P(),
            P(),
            P(),
            P(),
            P(),
            P(),
            P(),
            P(None, "ep"),
            P(),
            P("ep", None, None),
            P("ep", None, None),
            P("ep", None, None),
            P("ep", None),
            P("ep", None),
        ),
        out_specs=(P("ep", None), P("ep", None, None)),
        check_vma=False,
    )
```

time: 345 us -> 163 us (0.47); the launches traced: 338 us -> 162 us
  Pallas kernels: 0 us -> 131 us
  waiting for transfers between devices: 102 us -> 0 us
  local copies, waits for them, and re-layouts: 81.3 us -> 16.8 us
  matrix products: 65.2 us -> 8.37 us
  other arithmetic: 41.3 us -> 4.92 us
  starting transfers between devices: 33.9 us -> 0 us
  between operations: 14.5 us -> 1.01 us
    pallas_call x0 -> x5, Pallas kernels: none -> 131 us  [the longest x2 68.1 us: project(): pl.pallas_call(functools.partial(project_kernel, devices), out_shape=jax....]
    all_gather x2 -> x0, waiting for transfers between devices: 86.9 us -> none  [the longest x1 55.2 us: local(): lax.all_gather(normed, 'ep', axis=0, tiled=True)]
    mul x10 -> x0, local copies, waits for them, and re-layouts: 54.7 us -> none  [the longest x3 21.8 us: memory_readout(): memory_grid * forget_multiplier[:, :, None, :]]
    dot_general x4 -> x0, matrix products: 54.1 us -> none  [the longest x1 28.7 us: memory_readout(): jnp.einsum('bhij,bhj->bhi', memory_grid, erase_signal, precision=highest)]
    all_to_all x6 -> x0, starting transfers between devices: 33.7 us -> none  [the longest x1 5.86 us: local(): lax.all_to_all(results.reshape(received.shape), 'ep', split_axis=0, conca...]
    mul x4 -> x0, other arithmetic: 20.6 us -> none  [the longest x1 9.34 us: memory_readout(): content_signals[..., None] * substitute_lookup[:, :, None, :]]
    reshape x6 -> x7, local copies, waits for them, and re-layouts: 19.1 us -> 0.67 us  [the longest x4 0.28 us: local(): gain.reshape(attender_count, channel_span)]
    add x1 -> x0, other arithmetic: 16.1 us -> none  [memory_readout(): memory_grid * forget_multiplier[:, :, None, :]]
  transfers between devices with their start and end apart: 8 -> 0, of which waited for: 5 -> 0; matrix products, arithmetic and copies ran while one was open for 41% -> 0% of each run, Pallas kernels for 0% -> 0%
where the time goes in v1:
time: 163 us; the launch traced here: 162 us
  Pallas kernels  131 us (80%)
  local copies, waits for them, and re-layouts  16.8 us (10%)
  matrix products  8.37 us (5%)
  other arithmetic  4.92 us (3%)
    pallas_call x2, Pallas kernels, project(): pl.pallas_call(functools.partial(project_kernel, devices), out_shape=jax....  68.1 us
    pallas_call x2, Pallas kernels, exchange(): pl.pallas_call(functools.partial(exchange_kernel, devices), out_shape=jax...  52.7 us
    pallas_call x1, Pallas kernels, update_state(): pl.pallas_call(state_kernel, grid=(seqs * heads // block,), in_specs=[row...  10.1 us
    unnamed x35, local copies, waits for them, and re-layouts  8.23 us
    dot_general x1, matrix products, local(): jnp.dot(hidden_act, specialist_shrink_maps[0], preferred_element_type=jnp...  3.59 us
    another operation x2, local copies, waits for them, and re-layouts, exchange(): blocks = x.reshape(devices, -1, 128)  3.44 us

profile of v1, /device:TPU:15, one launch (start us, length us, event | category | flops | bytes accessed | tf_op | source)
XLA Modules:
  0.0 162.1 jit_solution(17488391373436701593)
XLA Ops:
  0.6 1.1 fusion.21
  1.8 0.9 fusion.23.x_ref
  2.7 1.2 copy.45
  3.9 1.2 copy.46
  5.2 2.0 %copy.47 = bf16[2048,64]{1,0:T(8,128)(2,1)} copy(bf16[2048,64]{0,1:T(8,128)(2,1)} %param.28) | data formatting | bytes 524288 | tf_op args[5]
  7.1 1.6 pad_maximum_fusion.w_ref
  8.7 35.9 %project0.1 = bf16[16,2,16,192]{3,2,1,0:T(8,128)(2,1)S(1)} custom-call(bf16[16,2048]{1,0:T(8,128)(2,1)S(1)} %fusion.23.x_ref, bf16[2048,192]{1,0:T(8,128)(2,1)S(1)} %pad_maximum_fusion.w_ref), custom_call_target="tpu_custom_call" | custom-call | tf_op jit(solution)/shard_map/project0/pallas_call | solution.py:209
  44.6 0.1 reshape_reshape.15
  44.8 0.6 fusion.36
  45.7 0.4 convolution_add_fusion.1
  46.2 1.4 convolution_add_fusion
  48.0 3.4 %copy-done.1 = f32[16,32,4096]{2,1,0:T(8,128)S(1)} copy-done((f32[16,32,4096]{2,1,0:T(8,128)S(1)}, f32[16,32,4096]{2,1,0:T(8,128)}, u32[]{:S(2)}) %copy-start.1) | copy-done | bytes 8388632
  51.4 10.1 %state.1 = (bf16[512,64]{1,0:T(8,128)(2,1)S(1)}, f32[512,4096]{1,0:T(8,128)}) custom-call(bf16[512,64]{1,0:T(8,128)(2,1)S(1)} %bitcast.42, bf16[512,64]{1,0:T(8,128)(2,1)S(1)} %bitcast.43, bf16[512,64]{1,0:T(8,128)(2,1)S(1)} %bitcast.44, f32[512,64]{1,0:T(8,128)S(1)} %reshape.103.dl_ref, f32[512,64]{1,0:T(8,128)S(1)} %reshape.104.al_ref, ...), custom_call_target="tpu_custom_call" | custom-call | tf_op jit(solution)/shard_map/state/pallas_call | solution.py:101
  61.5 0.2 reshape.110.x_ref
  61.7 0.3 copy.51.w_ref
  62.0 32.2 %project1.1 = bf16[16,2,16,64]{3,2,1,0:T(8,128)(2,1)S(1)} custom-call(bf16[16,2048]{1,0:T(8,128)(2,1)S(1)} %reshape.110.x_ref, bf16[2048,64]{1,0:T(8,128)(2,1)S(1)} %copy.51.w_ref), custom_call_target="tpu_custom_call" | custom-call | tf_op jit(solution)/shard_map/project1/pallas_call | solution.py:209
  94.4 0.1 reshape.113
  94.5 0.1 fusion.25
  94.8 0.1 reshape.111
  95.2 0.1 reduce_window_sum.11
  95.4 0.2 select_reduce_fusion
  95.6 0.5 convolution_convert_fusion.1
  96.1 1.2 reshape_reshape.16.x_ref
  97.3 28.8 %exchange2.1 = bf16[32,96,128]{2,1,0:T(8,128)(2,1)} custom-call(bf16[32,96,128]{2,1,0:T(8,128)(2,1)} %reshape_reshape.16.x_ref), custom_call_target="tpu_custom_call" | custom-call | tf_op jit(solution)/shard_map/exchange2/pallas_call | solution.py:278
  126.1 1.4 reshape_reshape.17
  127.5 2.2 %fusion.3 = f32[192,512]{1,0:T(8,128)S(1)} fusion(bf16[192,2048]{1,0:T(8,128)(2,1)S(1)} %reshape_reshape.17, bf16[1,2048,512]{2,1,0:T(8,128)(2,1)} %param.41), kind=kOutput, calls=%fused_computation.8 | convolution fusion | flops 402653184 | bytes 3276800 | tf_op jit(solution)/shard_map/dot_general | solution.py:386
  129.7 3.6 %convolution_convert_fusion = bf16[192,2048]{1,0:T(8,128)(2,1)} fusion(bf16[1,512,2048]{2,1,0:T(8,128)(2,1)S(1)} %copy-done, bf16[192,2048]{1,0:T(8,128)(2,1)S(1)} %reshape_reshape.17, bf16[1,2048,512]{2,1,0:T(8,128)(2,1)} %param.42, f32[192,512]{1,0:T(8,128)S(1)} %fusion.3), kind=kOutput, calls=%fused_computation | convolution fusion | flops 806289408 | bytes 6160384 | tf_op jit(solution)/shard_map/dot_general | solution.py:389
  133.3 2.2 %reshape_reshape.18.x_ref = bf16[32,96,128]{2,1,0:T(8,128)(2,1)} reshape(bf16[192,2048]{1,0:T(8,128)(2,1)} %convolution_convert_fusion) | data formatting | bytes 1572864 | tf_op jit(solution)/shard_map/reshape;reshape | solution.py:277
  135.5 24.0 %exchange3.1 = bf16[32,96,128]{2,1,0:T(8,128)(2,1)} custom-call(bf16[32,96,128]{2,1,0:T(8,128)(2,1)} %reshape_reshape.18.x_ref), custom_call_target="tpu_custom_call" | custom-call | tf_op jit(solution)/shard_map/exchange3/pallas_call | solution.py:278
  159.5 1.4 reshape.115
  161.1 0.3 fusion.5
  161.4 0.6 fusion.28
  (51 shorter events, 1.5 us)
Async XLA Ops:
  0.6 129.1 %copy-start = (bf16[1,512,2048]{2,1,0:T(8,128)(2,1)S(1)}, bf16[1,512,2048]{2,1,0:T(8,128)(2,1)}, u32[]{:S(2)}) copy-start(bf16[1,512,2048]{2,1,0:T(8,128)(2,1)} %param.43) | copy-start | bytes 6291460
  44.6 1.1 copy-start.4
  44.6 1.1 copy-start.5
  44.6 1.1 copy-start.7
  44.7 1.4 copy-start.8
  45.3 2.4 %copy-start.9 = (f32[2048]{0:T(1024)S(1)}, f32[2048]{0:T(1024)}, u32[]{:S(2)}) copy-start(f32[2048]{0:T(1024)} %param.35) | copy-start | bytes 24580
  45.3 2.5 %copy-start.10 = (f32[2048]{0:T(1024)S(1)}, f32[2048]{0:T(1024)}, u32[]{:S(2)}) copy-start(f32[2048]{0:T(1024)} %param.36) | copy-start | bytes 24580
  45.3 2.5 %copy-start.11 = (f32[2048]{0:T(1024)S(1)}, f32[2048]{0:T(1024)}, u32[]{:S(2)}) copy-start(f32[2048]{0:T(1024)} %param.37) | copy-start | bytes 24580
  45.4 2.6 %copy-start.12 = (f32[2048]{0:T(1024)S(1)}, f32[2048]{0:T(1024)}, u32[]{:S(2)}) copy-start(f32[2048]{0:T(1024)} %param.38) | copy-start | bytes 24580
  48.0 3.4 %copy-start.1 = (f32[16,32,4096]{2,1,0:T(8,128)S(1)}, f32[16,32,4096]{2,1,0:T(8,128)}, u32[]{:S(2)}) copy-start(f32[16,32,4096]{2,1,0:T(8,128)} %param.24) | copy-start | bytes 25165828
  51.4 10.3 %copy-start.3 = (bf16[2048,64]{0,1:T(8,128)(2,1)S(1)}, bf16[2048,64]{0,1:T(8,128)(2,1)}, u32[]{:S(2)}) copy-start(bf16[2048,64]{0,1:T(8,128)(2,1)} %param.39) | copy-start | bytes 786436
  61.5 33.0 %copy-start.2 = (bf16[16,2048]{1,0:T(8,128)(2,1)S(1)}, bf16[16,2048]{1,0:T(8,128)(2,1)}, u32[]{:S(2)}) copy-start(bf16[16,2048]{1,0:T(8,128)(2,1)} %param.23) | copy-start | bytes 196612
  61.5 33.1 %copy-start.13 = (f32[2048]{0:T(1024)S(1)}, f32[2048]{0:T(1024)}, u32[]{:S(2)}) copy-start(f32[2048]{0:T(1024)} %param.40) | copy-start | bytes 24580
  62.0 33.0 %copy-start.6 = (s32[16,6]{0,1:T(8,128)S(1)}, s32[16,6]{0,1:T(8,128)}, u32[]{:S(2)}) copy-start(s32[16,6]{0,1:T(8,128)} %param.44) | copy-start | bytes 1156
  133.3 27.8 %copy-start.14 = (f32[16,6]{0,1:T(8,128)S(1)}, f32[16,6]{0,1:T(8,128)}, u32[]{:S(2)}) copy-start(f32[16,6]{0,1:T(8,128)} %param.45) | copy-start | bytes 1156

commit v2 on v1

--- a/solution.py
+++ b/solution.py
@@ -10,6 +10,7 @@
 
 GROUPS = 4
 MESH = pl.DeviceIdType.MESH
+OUTER = 4
 
 norm_eps = 1e-06
 group_eps = 0.00064
@@ -111,7 +112,7 @@
             pltpu.VMEM((cells, span), jnp.bfloat16),
             pltpu.VMEM((2 * span, cells), jnp.bfloat16),
         ],
-        compiler_params=pltpu.CompilerParams(vmem_limit_bytes=40 * 2**20),
+        compiler_params=pltpu.CompilerParams(vmem_limit_bytes=16 * 2**20),
         name="state",
     )(q, k, v, decay_logit, rate_logit, *gains, state.reshape(seqs * heads, cells))
     return mixed, new.reshape(state.shape)
@@ -119,7 +120,7 @@
 
 def project_kernel(
     devices, x_ref, w_ref, out_ref, gathered, other, result, landed,
-    x_send, x_recv, r_send, r_recv, w_send, w_recv, local_sem,
+    z_send, z_recv, x_send, x_recv, r_send, r_recv, w_send, w_recv, local_sem,
 ):
     me = lax.axis_index("ep")
     core, chip = me % 2, me // 2
@@ -138,15 +139,44 @@
     lax.fori_loop(1, chips, greet, 0)
     pl.semaphore_wait(barrier, chips)
 
-    def token_copy(k):
+    inner = chips // OUTER
+    layer, place = chip // inner, chip % inner
+
+    def block_of(j):
+        return ((layer + OUTER - j) % OUTER) * inner + place
+
+    def outer_copy(j):
         return pltpu.make_async_remote_copy(
             src_ref=x_ref,
             dst_ref=gathered.at[chip],
-            send_sem=x_send.at[k],
-            recv_sem=x_recv.at[k],
-            device_id=((me + 2 * k) % devices,),
+            send_sem=z_send.at[j],
+            recv_sem=z_recv.at[j],
+            device_id=((((layer + j) % OUTER) * inner + place) * 2 + core,),
             device_id_type=MESH,
         )
+
+    def inner_copy(j, r):
+        block = gathered.at[block_of(j)]
+        return pltpu.make_async_remote_copy(
+            src_ref=x_ref if j == 0 else block,
+            dst_ref=block,
+            send_sem=x_send.at[j, r],
+            recv_sem=x_recv.at[j, r],
+            device_id=((layer * inner + (place + r) % inner) * 2 + core,),
+            device_id_type=MESH,
+        )
+
+    def inner_start(j):
+        def step(r, carry):
+            inner_copy(j, r).start()
+            return carry
+        lax.fori_loop(1, inner, step, 0)
+
+    def inner_finish(j):
+        def step(r, carry):
+            inner_copy(j, r).wait()
+            return carry
+        lax.fori_loop(1, inner, step, 0)
 
     def result_copy(k):
         peer = (me + 2 * k) % devices
@@ -179,16 +209,26 @@
         device_id=(partner,),
         device_id_type=MESH,
     )
-    start(token_copy)
+    for j in range(1, OUTER):
+        outer_copy(j).start()
+    inner_start(0)
     weights.start()
     mine = pltpu.make_async_copy(x_ref, gathered.at[chip], local_sem)
     mine.start()
     mine.wait()
+    for j in range(1, OUTER):
+        outer_copy(j).wait_recv()
+        inner_start(j)
     weights.wait()
-    finish(token_copy)
+    for j in range(1, OUTER):
+        outer_copy(j).wait_send()
+    for j in range(OUTER):
+        inner_finish(j)
     tokens = gathered[...].reshape(chips * rows, x_ref.shape[1])
     for ref, at in ((w_ref, core), (other, 1 - core)):
-        product = jnp.dot(tokens, ref[...], preferred_element_type=jnp.float32)
+        product = lax.dot_general(
+            tokens, ref[...], (((1,), (1,)), ((), ())), preferred_element_type=jnp.float32
+        )
         product = product.astype(jnp.bfloat16)
         for c in range(chips):
             result[c, at] = product[c * rows : (c + 1) * rows]
@@ -204,7 +244,7 @@
     devices = lax.axis_size("ep")
     chips = devices // 2
     rows, depth = x.shape
-    columns = w.shape[1]
+    columns = w.shape[0]
     shape = (chips, 2, rows, columns)
     out = pl.pallas_call(
         functools.partial(project_kernel, devices),
@@ -216,8 +256,10 @@
             pltpu.VMEM(w.shape, jnp.bfloat16),
             pltpu.VMEM(shape, jnp.bfloat16),
             pltpu.VMEM(shape, jnp.bfloat16),
-            pltpu.SemaphoreType.DMA((chips,)),
-            pltpu.SemaphoreType.DMA((chips,)),
+            pltpu.SemaphoreType.DMA((OUTER,)),
+            pltpu.SemaphoreType.DMA((OUTER,)),
+            pltpu.SemaphoreType.DMA((OUTER, chips // OUTER)),
+            pltpu.SemaphoreType.DMA((OUTER, chips // OUTER)),
             pltpu.SemaphoreType.DMA((chips,)),
             pltpu.SemaphoreType.DMA((chips,)),
             pltpu.SemaphoreType.DMA,
@@ -225,7 +267,12 @@
             pltpu.SemaphoreType.DMA,
         ],
         compiler_params=pltpu.CompilerParams(
-            collective_id=ident, has_side_effects=True, vmem_limit_bytes=50 * 2**20
+            collective_id=ident, has_side_effects=True, vmem_limit_bytes=20 * 2**20
+        ),
+        cost_estimate=pl.CostEstimate(
+            flops=4 * chips * rows * depth * columns,
+            bytes_accessed=32 * chips * rows * depth * 2,
+            transcendentals=0,
         ),
         name=f"project{ident}",
     )(x, w)
@@ -323,7 +370,7 @@
     devices = lax.axis_size("ep")
     columns = query_map.shape[1]
     normed = rms_norm(latest_embeddings, earlier_rescale_gain)
-    stacked = jnp.concatenate([query_map, lookup_map, content_map], axis=1)
+    stacked = jnp.concatenate([query_map.T, lookup_map.T, content_map.T], axis=0)
     projected = project(normed, stacked, 0).reshape(devices, seq_count, 3, columns)
     projected = projected.transpose(2, 1, 0, 3).reshape(
         3, seq_count * attender_count, channel_span
@@ -357,7 +404,7 @@
         ],
         prior_memory_grids,
     )
-    mixer_out = project(mixed.reshape(seq_count, model_width), result_map, 1)
+    mixer_out = project(mixed.reshape(seq_count, model_width), result_map.T, 1)
     mixer_out = mixer_out.transpose(1, 0, 2).reshape(seq_count, model_width)
     residual = (latest_embeddings.astype(jnp.float32) + mixer_out.astype(jnp.float32)).astype(
         jnp.bfloat16

time: 163 us -> 135 us (0.83)
  Pallas kernels: 131 us -> 108 us
  local copies, waits for them, and re-layouts: 16.8 us -> 12.1 us
    pallas_call x2, Pallas kernels: 68.1 us -> 44.2 us  [project(): pl.pallas_call(functools.partial(project_kernel, devices), out_shape=jax....]
    unnamed x35 -> x31, local copies, waits for them, and re-layouts: 8.23 us -> 3.55 us
where the time goes in v2:
time: 135 us; the launch traced here: 134 us
  Pallas kernels  108 us (80%)
  local copies, waits for them, and re-layouts  12.1 us (9%)
  matrix products  8.37 us (6%)
  other arithmetic  4.54 us (3%)
    pallas_call x2, Pallas kernels, exchange(): pl.pallas_call(functools.partial(exchange_kernel, devices), out_shape=jax...  53.9 us
    pallas_call x2, Pallas kernels, project(): pl.pallas_call(functools.partial(project_kernel, devices), out_shape=jax....  44.2 us
    pallas_call x1, Pallas kernels, update_state(): pl.pallas_call(state_kernel, grid=(seqs * heads // block,), in_specs=[row...  10.1 us
    dot_general x1, matrix products, local(): jnp.dot(hidden_act, specialist_shrink_maps[0], preferred_element_type=jnp...  3.59 us
    unnamed x31, local copies, waits for them, and re-layouts  3.55 us
    another operation x2, local copies, waits for them, and re-layouts, exchange(): blocks = x.reshape(devices, -1, 128)  3.44 us

profile of v2, /device:TPU:15, one launch (start us, length us, event | category | flops | bytes accessed | tf_op | source)
XLA Modules:
  0.0 134.2 jit_solution(4547144966178372557)
XLA Ops:
  0.6 1.1 fusion.21
  1.8 0.9 fusion.23.x_ref
  2.7 1.2 pad_maximum_fusion.w_ref
  3.9 21.6 %project0.1 = bf16[16,2,16,192]{3,2,1,0:T(8,128)(2,1)S(1)} custom-call(bf16[16,2048]{1,0:T(8,128)(2,1)S(1)} %fusion.23.x_ref, bf16[192,2048]{1,0:T(8,128)(2,1)S(1)} %pad_maximum_fusion.w_ref), custom_call_target="tpu_custom_call" | custom-call | flops 402653184 | bytes 33554432 | tf_op jit(solution)/shard_map/project0/pallas_call | solution.py:249
  25.6 0.1 reshape_reshape.15
  25.7 0.6 fusion.36
  26.3 0.1 copy.37
  26.4 0.1 copy.38
  26.7 0.4 convolution_add_fusion.1
  27.1 0.1 reshape.103.dl_ref
  27.2 1.4 %convolution_add_fusion = f32[16,2048]{1,0:T(8,128)S(1)} fusion(bf16[64,2048]{1,0:T(8,128)(2,1)} %param.33, bf16[16,2048]{1,0:T(8,128)(2,1)S(1)} %fusion.23.x_ref, bf16[2048,64]{0,1:T(8,128)(2,1)} %param.32, f32[2048]{0:T(1024)S(1)} %copy-done.8), kind=kOutput, calls=%fused_computation.3 | convolution fusion | flops 8422400 | bytes 729088 | tf_op jit(solution)/shard_map/dot_general | solution.py:387
  28.6 0.1 reshape.104.al_ref
  29.0 3.4 %copy-done.1 = f32[16,32,4096]{2,1,0:T(8,128)S(1)} copy-done((f32[16,32,4096]{2,1,0:T(8,128)S(1)}, f32[16,32,4096]{2,1,0:T(8,128)}, u32[]{:S(2)}) %copy-start.1) | copy-done | bytes 8388632
  32.4 10.1 %state.1 = (bf16[512,64]{1,0:T(8,128)(2,1)S(1)}, f32[512,4096]{1,0:T(8,128)}) custom-call(bf16[512,64]{1,0:T(8,128)(2,1)S(1)} %bitcast.46, bf16[512,64]{1,0:T(8,128)(2,1)S(1)} %bitcast.47, bf16[512,64]{1,0:T(8,128)(2,1)S(1)} %bitcast.48, f32[512,64]{1,0:T(8,128)S(1)} %reshape.103.dl_ref, f32[512,64]{1,0:T(8,128)S(1)} %reshape.104.al_ref, ...), custom_call_target="tpu_custom_call" | custom-call | tf_op jit(solution)/shard_map/state/pallas_call | solution.py:102
  42.5 0.2 reshape.110.x_ref
  42.7 22.6 %project1.1 = bf16[16,2,16,64]{3,2,1,0:T(8,128)(2,1)S(1)} custom-call(bf16[16,2048]{1,0:T(8,128)(2,1)S(1)} %reshape.110.x_ref, bf16[64,2048]{1,0:T(8,128)(2,1)S(1)} %bitcast.49), custom_call_target="tpu_custom_call" | custom-call | flops 134217728 | bytes 33554432 | tf_op jit(solution)/shard_map/project1/pallas_call | solution.py:249
  65.4 0.1 reshape.113
  65.5 0.1 fusion.25
  65.8 0.1 reshape.111
  66.3 0.1 reduce_window_sum.11
  66.4 0.2 select_reduce_fusion
  66.6 0.5 convolution_convert_fusion.1
  67.1 1.2 reshape_reshape.16.x_ref
  68.3 29.2 %exchange2.1 = bf16[32,96,128]{2,1,0:T(8,128)(2,1)} custom-call(bf16[32,96,128]{2,1,0:T(8,128)(2,1)} %reshape_reshape.16.x_ref), custom_call_target="tpu_custom_call" | custom-call | tf_op jit(solution)/shard_map/exchange2/pallas_call | solution.py:325
  97.5 1.4 %reshape_reshape.17 = bf16[192,2048]{1,0:T(8,128)(2,1)S(1)} reshape(bf16[32,96,128]{2,1,0:T(8,128)(2,1)} %exchange2.1) | data formatting | bytes 1572864 | tf_op jit(solution)/shard_map/reshape;reshape | solution.py:432
  99.0 2.2 %fusion.3 = f32[192,512]{1,0:T(8,128)S(1)} fusion(bf16[192,2048]{1,0:T(8,128)(2,1)S(1)} %reshape_reshape.17, bf16[1,2048,512]{2,1,0:T(8,128)(2,1)} %param.41), kind=kOutput, calls=%fused_computation.8 | convolution fusion | flops 402653184 | bytes 3276800 | tf_op jit(solution)/shard_map/dot_general | solution.py:433
  101.1 3.6 %convolution_convert_fusion = bf16[192,2048]{1,0:T(8,128)(2,1)} fusion(bf16[1,512,2048]{2,1,0:T(8,128)(2,1)S(1)} %copy-done, bf16[192,2048]{1,0:T(8,128)(2,1)S(1)} %reshape_reshape.17, bf16[1,2048,512]{2,1,0:T(8,128)(2,1)} %param.42, f32[192,512]{1,0:T(8,128)S(1)} %fusion.3), kind=kOutput, calls=%fused_computation | convolution fusion | flops 806289408 | bytes 6160384 | tf_op jit(solution)/shard_map/dot_general | solution.py:436
  104.7 2.2 %reshape_reshape.18.x_ref = bf16[32,96,128]{2,1,0:T(8,128)(2,1)} reshape(bf16[192,2048]{1,0:T(8,128)(2,1)} %convolution_convert_fusion) | data formatting | bytes 1572864 | tf_op jit(solution)/shard_map/reshape;reshape | solution.py:324
  106.9 24.7 %exchange3.1 = bf16[32,96,128]{2,1,0:T(8,128)(2,1)} custom-call(bf16[32,96,128]{2,1,0:T(8,128)(2,1)} %reshape_reshape.18.x_ref), custom_call_target="tpu_custom_call" | custom-call | tf_op jit(solution)/shard_map/exchange3/pallas_call | solution.py:325
  131.6 1.4 %reshape.115 = bf16[192,2048,1]{1,0,2:T(8,128)(2,1)S(1)} reshape(bf16[32,96,128]{2,1,0:T(8,128)(2,1)} %exchange3.1) | data formatting | bytes 1572864 | tf_op jit(solution)/shard_map/reshape;reshape | solution.py:441
  133.2 0.3 fusion.5
  133.6 0.6 fusion.28
  (47 shorter events, 1.2 us)
Async XLA Ops:
  0.6 100.5 %copy-start = (bf16[1,512,2048]{2,1,0:T(8,128)(2,1)S(1)}, bf16[1,512,2048]{2,1,0:T(8,128)(2,1)}, u32[]{:S(2)}) copy-start(bf16[1,512,2048]{2,1,0:T(8,128)(2,1)} %param.43) | copy-start | bytes 6291460
  25.5 1.1 copy-start.4
  25.5 1.1 copy-start.5
  25.5 1.1 copy-start.7
  25.7 1.4 %copy-start.8 = (f32[2048]{0:T(1024)S(1)}, f32[2048]{0:T(1024)}, u32[]{:S(2)}) copy-start(f32[2048]{0:T(1024)} %param.34) | copy-start | bytes 24580
  26.3 2.4 %copy-start.9 = (f32[2048]{0:T(1024)S(1)}, f32[2048]{0:T(1024)}, u32[]{:S(2)}) copy-start(f32[2048]{0:T(1024)} %param.35) | copy-start | bytes 24580
  26.3 2.5 %copy-start.10 = (f32[2048]{0:T(1024)S(1)}, f32[2048]{0:T(1024)}, u32[]{:S(2)}) copy-start(f32[2048]{0:T(1024)} %param.36) | copy-start | bytes 24580
  26.3 2.5 %copy-start.11 = (f32[2048]{0:T(1024)S(1)}, f32[2048]{0:T(1024)}, u32[]{:S(2)}) copy-start(f32[2048]{0:T(1024)} %param.37) | copy-start | bytes 24580
  26.3 2.6 %copy-start.12 = (f32[2048]{0:T(1024)S(1)}, f32[2048]{0:T(1024)}, u32[]{:S(2)}) copy-start(f32[2048]{0:T(1024)} %param.38) | copy-start | bytes 24580
  29.0 3.4 %copy-start.1 = (f32[16,32,4096]{2,1,0:T(8,128)S(1)}, f32[16,32,4096]{2,1,0:T(8,128)}, u32[]{:S(2)}) copy-start(f32[16,32,4096]{2,1,0:T(8,128)} %param.24) | copy-start | bytes 25165828
  32.4 10.3 %copy-start.2 = (bf16[2048,64]{0,1:T(8,128)(2,1)S(1)}, bf16[2048,64]{0,1:T(8,128)(2,1)}, u32[]{:S(2)}) copy-start(bf16[2048,64]{0,1:T(8,128)(2,1)} %param.39) | copy-start | bytes 786436
  32.4 33.1 %copy-start.3 = (bf16[16,2048]{1,0:T(8,128)(2,1)S(1)}, bf16[16,2048]{1,0:T(8,128)(2,1)}, u32[]{:S(2)}) copy-start(bf16[16,2048]{1,0:T(8,128)(2,1)} %param.23) | copy-start | bytes 196612
  42.5 23.2 %copy-start.13 = (f32[2048]{0:T(1024)S(1)}, f32[2048]{0:T(1024)}, u32[]{:S(2)}) copy-start(f32[2048]{0:T(1024)} %param.40) | copy-start | bytes 24580
  42.5 23.5 %copy-start.6 = (s32[16,6]{0,1:T(8,128)S(1)}, s32[16,6]{0,1:T(8,128)}, u32[]{:S(2)}) copy-start(s32[16,6]{0,1:T(8,128)} %param.44) | copy-start | bytes 1156
  104.7 28.5 %copy-start.14 = (f32[16,6]{0,1:T(8,128)S(1)}, f32[16,6]{0,1:T(8,128)}, u32[]{:S(2)}) copy-start(f32[16,6]{0,1:T(8,128)} %param.45) | copy-start | bytes 1156

commit v3 on v2

--- a/solution.py
+++ b/solution.py
@@ -224,14 +224,15 @@
         outer_copy(j).wait_send()
     for j in range(OUTER):
         inner_finish(j)
-    tokens = gathered[...].reshape(chips * rows, x_ref.shape[1])
-    for ref, at in ((w_ref, core), (other, 1 - core)):
-        product = lax.dot_general(
-            tokens, ref[...], (((1,), (1,)), ((), ())), preferred_element_type=jnp.float32
-        )
-        product = product.astype(jnp.bfloat16)
-        for c in range(chips):
-            result[c, at] = product[c * rows : (c + 1) * rows]
+        base = ((layer + OUTER - j) % OUTER) * inner
+        tokens = gathered[pl.ds(base, inner)].reshape(inner * rows, x_ref.shape[1])
+        for ref, at in ((w_ref, core), (other, 1 - core)):
+            product = lax.dot_general(
+                tokens, ref[...], (((1,), (1,)), ((), ())), preferred_element_type=jnp.float32
+            )
+            product = product.astype(jnp.bfloat16)
+            for c in range(inner):
+                result[base + c, at] = product[c * rows : (c + 1) * rows]
     start(result_copy)
     mine = pltpu.make_async_copy(result.at[chip], landed.at[chip], local_sem)
     mine.start()

time: 135 us -> 134 us (level)
  no operation moved by 1% of the time
where the time goes in v3:
time: 134 us
  Pallas kernels  108 us (81%)
  local copies, waits for them, and re-layouts  12.1 us (9%)
  matrix products  8.37 us (6%)
  other arithmetic  4.54 us (3%)
    pallas_call x2, Pallas kernels, exchange(): pl.pallas_call(functools.partial(exchange_kernel, devices), out_shape=jax...  54 us
    pallas_call x2, Pallas kernels, project(): pl.pallas_call(functools.partial(project_kernel, devices), out_shape=jax....  43.7 us
    pallas_call x1, Pallas kernels, update_state(): pl.pallas_call(state_kernel, grid=(seqs * heads // block,), in_specs=[row...  10.1 us
    dot_general x1, matrix products, local(): jnp.dot(hidden_act, specialist_shrink_maps[0], preferred_element_type=jnp...  3.59 us
    unnamed x31, local copies, waits for them, and re-layouts  3.55 us
    another operation x2, local copies, waits for them, and re-layouts, exchange(): blocks = x.reshape(devices, -1, 128)  3.44 us

profile of v3, /device:TPU:15, one launch (start us, length us, event | category | flops | bytes accessed | tf_op | source)
XLA Modules:
  0.0 133.8 jit_solution(10058981947873117228)
XLA Ops:
  0.6 1.1 fusion.21
  1.8 0.9 fusion.23.x_ref
  2.7 1.2 pad_maximum_fusion.w_ref
  3.9 21.5 %project0.1 = bf16[16,2,16,192]{3,2,1,0:T(8,128)(2,1)S(1)} custom-call(bf16[16,2048]{1,0:T(8,128)(2,1)S(1)} %fusion.23.x_ref, bf16[192,2048]{1,0:T(8,128)(2,1)S(1)} %pad_maximum_fusion.w_ref), custom_call_target="tpu_custom_call" | custom-call | flops 402653184 | bytes 33554432 | tf_op jit(solution)/shard_map/project0/pallas_call | solution.py:250
  25.5 0.1 reshape_reshape.15
  25.6 0.6 fusion.36
  26.2 0.1 copy.37
  26.3 0.1 copy.38
  26.5 0.4 convolution_add_fusion.1
  26.9 0.1 reshape.103.dl_ref
  27.1 1.4 %convolution_add_fusion = f32[16,2048]{1,0:T(8,128)S(1)} fusion(bf16[64,2048]{1,0:T(8,128)(2,1)} %param.33, bf16[16,2048]{1,0:T(8,128)(2,1)S(1)} %fusion.23.x_ref, bf16[2048,64]{0,1:T(8,128)(2,1)} %param.32, f32[2048]{0:T(1024)S(1)} %copy-done.8), kind=kOutput, calls=%fused_computation.3 | convolution fusion | flops 8422400 | bytes 729088 | tf_op jit(solution)/shard_map/dot_general | solution.py:388
  28.5 0.1 reshape.104.al_ref
  28.9 3.4 %copy-done.1 = f32[16,32,4096]{2,1,0:T(8,128)S(1)} copy-done((f32[16,32,4096]{2,1,0:T(8,128)S(1)}, f32[16,32,4096]{2,1,0:T(8,128)}, u32[]{:S(2)}) %copy-start.1) | copy-done | bytes 8388632
  32.3 10.1 %state.1 = (bf16[512,64]{1,0:T(8,128)(2,1)S(1)}, f32[512,4096]{1,0:T(8,128)}) custom-call(bf16[512,64]{1,0:T(8,128)(2,1)S(1)} %bitcast.46, bf16[512,64]{1,0:T(8,128)(2,1)S(1)} %bitcast.47, bf16[512,64]{1,0:T(8,128)(2,1)S(1)} %bitcast.48, f32[512,64]{1,0:T(8,128)S(1)} %reshape.103.dl_ref, f32[512,64]{1,0:T(8,128)S(1)} %reshape.104.al_ref, ...), custom_call_target="tpu_custom_call" | custom-call | tf_op jit(solution)/shard_map/state/pallas_call | solution.py:102
  42.4 0.2 reshape.110.x_ref
  42.6 22.2 %project1.1 = bf16[16,2,16,64]{3,2,1,0:T(8,128)(2,1)S(1)} custom-call(bf16[16,2048]{1,0:T(8,128)(2,1)S(1)} %reshape.110.x_ref, bf16[64,2048]{1,0:T(8,128)(2,1)S(1)} %bitcast.49), custom_call_target="tpu_custom_call" | custom-call | flops 134217728 | bytes 33554432 | tf_op jit(solution)/shard_map/project1/pallas_call | solution.py:250
  64.9 0.1 reshape.113
  65.0 0.1 fusion.25
  65.3 0.1 reshape.111
  65.8 0.1 reduce_window_sum.11
  65.9 0.2 select_reduce_fusion
  66.1 0.5 convolution_convert_fusion.1
  66.6 1.2 reshape_reshape.16.x_ref
  67.8 29.4 %exchange2.1 = bf16[32,96,128]{2,1,0:T(8,128)(2,1)} custom-call(bf16[32,96,128]{2,1,0:T(8,128)(2,1)} %reshape_reshape.16.x_ref), custom_call_target="tpu_custom_call" | custom-call | tf_op jit(solution)/shard_map/exchange2/pallas_call | solution.py:326
  97.2 1.4 %reshape_reshape.17 = bf16[192,2048]{1,0:T(8,128)(2,1)S(1)} reshape(bf16[32,96,128]{2,1,0:T(8,128)(2,1)} %exchange2.1) | data formatting | bytes 1572864 | tf_op jit(solution)/shard_map/reshape;reshape | solution.py:433
  98.7 2.2 %fusion.3 = f32[192,512]{1,0:T(8,128)S(1)} fusion(bf16[192,2048]{1,0:T(8,128)(2,1)S(1)} %reshape_reshape.17, bf16[1,2048,512]{2,1,0:T(8,128)(2,1)} %param.41), kind=kOutput, calls=%fused_computation.8 | convolution fusion | flops 402653184 | bytes 3276800 | tf_op jit(solution)/shard_map/dot_general | solution.py:434
  100.9 3.6 %convolution_convert_fusion = bf16[192,2048]{1,0:T(8,128)(2,1)} fusion(bf16[1,512,2048]{2,1,0:T(8,128)(2,1)S(1)} %copy-done, bf16[192,2048]{1,0:T(8,128)(2,1)S(1)} %reshape_reshape.17, bf16[1,2048,512]{2,1,0:T(8,128)(2,1)} %param.42, f32[192,512]{1,0:T(8,128)S(1)} %fusion.3), kind=kOutput, calls=%fused_computation | convolution fusion | flops 806289408 | bytes 6160384 | tf_op jit(solution)/shard_map/dot_general | solution.py:437
  104.5 2.2 %reshape_reshape.18.x_ref = bf16[32,96,128]{2,1,0:T(8,128)(2,1)} reshape(bf16[192,2048]{1,0:T(8,128)(2,1)} %convolution_convert_fusion) | data formatting | bytes 1572864 | tf_op jit(solution)/shard_map/reshape;reshape | solution.py:325
  106.6 24.6 %exchange3.1 = bf16[32,96,128]{2,1,0:T(8,128)(2,1)} custom-call(bf16[32,96,128]{2,1,0:T(8,128)(2,1)} %reshape_reshape.18.x_ref), custom_call_target="tpu_custom_call" | custom-call | tf_op jit(solution)/shard_map/exchange3/pallas_call | solution.py:326
  131.3 1.4 %reshape.115 = bf16[192,2048,1]{1,0,2:T(8,128)(2,1)S(1)} reshape(bf16[32,96,128]{2,1,0:T(8,128)(2,1)} %exchange3.1) | data formatting | bytes 1572864 | tf_op jit(solution)/shard_map/reshape;reshape | solution.py:442
  132.9 0.3 fusion.5
  133.2 0.6 fusion.28
  (47 shorter events, 1.2 us)
Async XLA Ops:
  0.6 100.2 %copy-start = (bf16[1,512,2048]{2,1,0:T(8,128)(2,1)S(1)}, bf16[1,512,2048]{2,1,0:T(8,128)(2,1)}, u32[]{:S(2)}) copy-start(bf16[1,512,2048]{2,1,0:T(8,128)(2,1)} %param.43) | copy-start | bytes 6291460
  25.4 1.1 copy-start.4
  25.4 1.1 copy-start.5
  25.4 1.1 copy-start.7
  25.6 1.4 %copy-start.8 = (f32[2048]{0:T(1024)S(1)}, f32[2048]{0:T(1024)}, u32[]{:S(2)}) copy-start(f32[2048]{0:T(1024)} %param.34) | copy-start | bytes 24580
  26.2 2.4 %copy-start.9 = (f32[2048]{0:T(1024)S(1)}, f32[2048]{0:T(1024)}, u32[]{:S(2)}) copy-start(f32[2048]{0:T(1024)} %param.35) | copy-start | bytes 24580
  26.2 2.5 %copy-start.10 = (f32[2048]{0:T(1024)S(1)}, f32[2048]{0:T(1024)}, u32[]{:S(2)}) copy-start(f32[2048]{0:T(1024)} %param.36) | copy-start | bytes 24580
  26.2 2.5 %copy-start.11 = (f32[2048]{0:T(1024)S(1)}, f32[2048]{0:T(1024)}, u32[]{:S(2)}) copy-start(f32[2048]{0:T(1024)} %param.37) | copy-start | bytes 24580
  26.2 2.6 %copy-start.12 = (f32[2048]{0:T(1024)S(1)}, f32[2048]{0:T(1024)}, u32[]{:S(2)}) copy-start(f32[2048]{0:T(1024)} %param.38) | copy-start | bytes 24580
  28.9 3.4 %copy-start.1 = (f32[16,32,4096]{2,1,0:T(8,128)S(1)}, f32[16,32,4096]{2,1,0:T(8,128)}, u32[]{:S(2)}) copy-start(f32[16,32,4096]{2,1,0:T(8,128)} %param.24) | copy-start | bytes 25165828
  32.3 10.3 %copy-start.2 = (bf16[2048,64]{0,1:T(8,128)(2,1)S(1)}, bf16[2048,64]{0,1:T(8,128)(2,1)}, u32[]{:S(2)}) copy-start(bf16[2048,64]{0,1:T(8,128)(2,1)} %param.39) | copy-start | bytes 786436
  32.3 32.7 %copy-start.3 = (bf16[16,2048]{1,0:T(8,128)(2,1)S(1)}, bf16[16,2048]{1,0:T(8,128)(2,1)}, u32[]{:S(2)}) copy-start(bf16[16,2048]{1,0:T(8,128)(2,1)} %param.23) | copy-start | bytes 196612
  42.4 22.8 %copy-start.13 = (f32[2048]{0:T(1024)S(1)}, f32[2048]{0:T(1024)}, u32[]{:S(2)}) copy-start(f32[2048]{0:T(1024)} %param.40) | copy-start | bytes 24580
  42.4 23.1 %copy-start.6 = (s32[16,6]{0,1:T(8,128)S(1)}, s32[16,6]{0,1:T(8,128)}, u32[]{:S(2)}) copy-start(s32[16,6]{0,1:T(8,128)} %param.44) | copy-start | bytes 1156
  104.5 28.4 %copy-start.14 = (f32[16,6]{0,1:T(8,128)S(1)}, f32[16,6]{0,1:T(8,128)}, u32[]{:S(2)}) copy-start(f32[16,6]{0,1:T(8,128)} %param.45) | copy-start | bytes 1156
